TPU v7x, 128 devices: a whole 4x4x4 slice. The times are simulated.
128 devices in a mesh: rep: 2 (over z_hi), fs: 32 (over z_lo, y, x), tp: 2 (over core).
Axes of the slice: x: 4, y: 4, z: 4 (z_hi: 2, z_lo: 2; z = z_hi * 2 + z_lo), core: 2. Of those that a mesh axis runs over, the one named last changes fastest.
Arguments:
- tokens: bfloat16 [49152, 2048], P(('rep', 'fs', 'tp')), may hold values from -6 to 6
- outer_weight: float32 [2048, 1536], P('fs', 'tp'), may hold values from -0.125 to 0.125
- inner_weight: float32 [2048, 1536], P('fs', 'tp'), may hold values from -0.125 to 0.125
- value_weight: float32 [2048, 1536], P('fs', 'tp'), may hold values from -0.125 to 0.125
- conv_taps: float32 [3, 1536], P(None, 'tp'), may hold values from -3 to 3
- mix_out: float32 [1536, 2048], P('tp', 'fs'), may hold values from -0.15625 to 0.15625
- norm_first: float32 [2048], replicated, may hold values from 0.1 to 1.9
- up_weight: float32 [2048, 4096], P('fs', 'tp'), may hold values from -0.125 to 0.125
- down_weight: float32 [4096, 2048], P('tp', 'fs'), may hold values from -0.09375 to 0.09375
- norm_second: float32 [2048], replicated, may hold values from 0.1 to 1.9
Outputs:
- encoded: bfloat16 [49152, 2048], P(('rep', 'fs', 'tp'))
All inputs are finite; a program needn't handle non-finite values.
Results may differ from a plain program's by a relative error of at most 0.015.
Values may be sent and summed in bfloat16 or wider, within the bound.
No kernel may reach another device: no remote copies, remote signals or barrier semaphores. Data moves between devices by JAX's collectives and lax.ppermute only.
A program may use at most 128 MiB of HBM per device.

v0:
```python
import jax
import jax.numpy as jnp
from jax import lax
from jax.sharding import Mesh
from jax.sharding import PartitionSpec as P

SEQ = 128
FS = ("fs_0", "fs_1", "fs_2")
REP_FS = ("rep", "fs_0", "fs_1", "fs_2")
REP_FS_TP = ("rep", "fs_0", "fs_1", "fs_2", "tp")
residual_scale = 2.0**0.25
norm_epsilon = 1e-05


def own_half(x, dim):
    length = x.shape[dim] // 2
    return lax.dynamic_slice_in_dim(x, lax.axis_index("rep") * length, length, dim)


def gathered_halves(x):
    full = lax.all_gather(x, REP_FS, axis=0, tiled=True)
    return full.reshape(2, -1, x.shape[1])


def sum_at_owner(x, axis):
    tiles = x.reshape(2, -1, x.shape[1])
    arrived = lax.all_to_all(tiles, axis, split_axis=0, concat_axis=0, tiled=True)
    return arrived.astype(jnp.float32).sum(axis=0)


def layer_norm(values, scaling):
    center = values - jnp.mean(values, axis=-1, keepdims=True)
    spread = jnp.mean(center * center, axis=-1, keepdims=True)
    return center * lax.rsqrt(spread + norm_epsilon) * scaling


def short_conv(product, conv_taps):
    places = jnp.arange(product.shape[0], dtype=jnp.int32) % SEQ
    blank = jnp.zeros((1, product.shape[1]), jnp.float32)
    before = jnp.concatenate([blank, product[:-1]], axis=0)
    after = jnp.concatenate([product[1:], blank], axis=0)
    before = jnp.where((places > 0)[:, None], before, 0.0)
    after = jnp.where((places < SEQ - 1)[:, None], after, 0.0)
    return conv_taps[0] * before + conv_taps[1] * product + conv_taps[2] * after


def dot(a, b):
    return jnp.dot(a, b, preferred_element_type=jnp.float32)


def dot_t(a, b):
    return lax.dot_general(a, b, (((1,), (1,)), ((), ())), preferred_element_type=jnp.float32)


def local(
    tokens,
    outer_weight,
    inner_weight,
    value_weight,
    conv_taps,
    mix_out,
    norm_first,
    up_weight,
    down_weight,
    norm_second,
):
    bf = jnp.bfloat16
    grouped = lax.all_gather(tokens, "tp", axis=0, tiled=True)
    into = jnp.concatenate(
        [own_half(w, 1).astype(bf) for w in (outer_weight, inner_weight, value_weight)], axis=1
    )
    into_full = gathered_halves(into)
    mixout_full = gathered_halves(own_half(mix_out, 0).astype(bf).T)
    up_full = gathered_halves(own_half(up_weight, 1).astype(bf))
    down_full = gathered_halves(own_half(down_weight, 0).astype(bf).T)
    width = into.shape[1] // 3
    mixing = 0.0
    for h in range(2):
        w = into_full[h]
        outer = dot(grouped, w[:, :width])
        inner = dot(grouped, w[:, width : 2 * width])
        value = dot(grouped, w[:, 2 * width :])
        taps = conv_taps[:, h * width : (h + 1) * width]
        mixed = (outer * short_conv(inner * value, taps)).astype(bf)
        mixing = mixing + dot_t(mixed, mixout_full[h])
    mixing = sum_at_owner(mixing.astype(bf), "tp")
    first = layer_norm(residual_scale * tokens.astype(jnp.float32) + mixing, norm_first).astype(bf)
    grouped_first = lax.all_gather(first, "tp", axis=0, tiled=True)
    lowered = 0.0
    for h in range(2):
        raised = jax.nn.relu(dot(grouped_first, up_full[h]))
        hidden = (raised * raised).astype(bf)
        lowered = lowered + dot_t(hidden, down_full[h])
    lowered = sum_at_owner(lowered.astype(bf), "tp")
    return layer_norm(residual_scale * first.astype(jnp.float32) + lowered, norm_second).astype(bf)


def solution(mesh):
    finer = Mesh(
        mesh.devices.reshape(mesh.shape["rep"], 2, 4, 4, mesh.shape["tp"]),
        ("rep", "fs_0", "fs_1", "fs_2", "tp"),
    )
    placed = (
        P(REP_FS_TP, None),
        P(FS, "tp"),
        P(FS, "tp"),
        P(FS, "tp"),
        P(None, "tp"),
        P("tp", FS),
        P(),
        P(FS, "tp"),
        P("tp", FS),
        P(),
    )
    return jax.shard_map(
        local, mesh=finer, in_specs=placed, out_specs=P(REP_FS_TP, None), check_vma=False
    )
```

profile of v0, /device:TPU:1, one launch (start us, length us, event | category | flops | bytes accessed | tf_op | source)
XLA Modules:
  0.0 385.9 jit_solution(15496005332504647773)
XLA Ops:
  6.5 0.7 all-gather.9.cloned.1.call-update
  7.3 0.0 all-gather.7.cloned.1.call-start
  7.3 0.9 dynamic-slice_convert_fusion.5
  8.2 1.0 dynamic-slice_convert_fusion.3
  9.2 0.7 pad_maximum_fusion
  9.8 0.0 all-gather.7.cloned.1.call-update
  9.9 0.0 all-gather.11.cloned.1.call-start
  9.9 1.5 fusion.87
  11.4 0.0 all-gather.11.cloned.1.call-update
  11.5 0.0 all-gather.15.cloned.1.call-start
  11.5 0.7 dynamic-slice_convert_fusion.1
  12.2 0.0 all-gather.15.cloned.1.call-update
  12.2 0.0 all-gather.13.cloned.1.call-start
  12.3 0.8 slice_reduce_fusion.2
  13.1 14.3 %all-gather.9.cloned.1.call-done = bf16[768,2048]{1,0:T(8,128)(2,1)} async-done(((bf16[384,2048]{1,0:T(8,128)(2,1)}), bf16[768,2048]{1,0:T(8,128)(2,1)}) %all-gather.9.cloned.1.call-update) | async-done | bytes 3145744 | tf_op jit(solution)/shard_map/all_gather | solution.py:68
  27.5 84.8 %all-gather.7.cloned.1.call-done = bf16[4096,1152]{1,0:T(8,128)(2,1)} async-done(((bf16[64,1152]{1,0:T(8,128)(2,1)}), bf16[4096,1152]{1,0:T(8,128)(2,1)}) %all-gather.7.cloned.1.call-update) | async-done | bytes 9437200 | tf_op jit(solution)/shard_map/all_gather | solution.py:21
  112.3 4.0 %fusion.23 = f32[384,768]{1,0:T(8,128)S(1)} fusion(bf16[768,2048]{1,0:T(8,128)(2,1)} %all-gather.9.cloned.1.call-done, bf16[4096,1152]{1,0:T(8,128)(2,1)} %all-gather.7.cloned.1.call-done), kind=kOutput, calls=%fused_computation.29 | convolution fusion | flops 1207959552 | bytes 5898240 | tf_op jit(solution)/shard_map/dot_general | solution.py:48
  116.3 2.9 fusion.50
  119.2 1.8 fusion.96
  121.0 2.9 fusion.15
  123.9 2.9 fusion.47
  126.8 1.8 fusion.95
  128.6 51.8 %all-gather.11.cloned.1.call-done = bf16[4096,384]{1,0:T(8,128)(2,1)} async-done(((bf16[64,384]{1,0:T(8,128)(2,1)}), bf16[4096,384]{1,0:T(8,128)(2,1)}) %all-gather.11.cloned.1.call-update) | async-done | bytes 3145744 | tf_op jit(solution)/shard_map/all_gather | solution.py:21
  180.3 10.2 %fusion.21 = f32[768,2048]{1,0:T(8,128)} fusion(bf16[4096,384]{1,0:T(8,128)(2,1)} %all-gather.11.cloned.1.call-done, bf16[768,2048]{1,0:T(8,128)(2,1)} %all-gather.9.cloned.1.call-done, bf16[4096,1152]{1,0:T(8,128)(2,1)} %all-gather.7.cloned.1.call-done, f32[767,384]{0,1:T(8,128)} %get-tuple-element.14, f32[768,384]{0,1:T(8,128)S(1)} %fusion.50, ...), kind=kOutput, calls=%fused_computation.27 | convolution fusion | flops 2418573312 | bytes 16128000 | tf_op jit(solution)/shard_map/dot_general | solution.py:52
  190.6 11.4 %add_convert_fusion.1 = bf16[768,2048]{1,0:T(8,128)(2,1)} fusion(f32[768,2048]{1,0:T(8,128)} %fusion.21, bf16[4096,384]{1,0:T(8,128)(2,1)} %all-gather.11.cloned.1.call-done, bf16[768,2048]{1,0:T(8,128)(2,1)} %all-gather.9.cloned.1.call-done, bf16[4096,1152]{1,0:T(8,128)(2,1)} %all-gather.7.cloned.1.call-done, f32[767,384]{0,1:T(8,128)} %get-tuple-element.12, ...), kind=kOutput, calls=%fused_computation.3 | convolution fusion | flops 2421719040 | bytes 19273728 | tf_op jit(solution)/shard_map/dot_general | solution.py:52
  201.9 9.3 %all_to_all.10 = bf16[2,384,2048]{2,1,0:T(8,128)(2,1)S(1)} all-to-all(bf16[2,384,2048]{2,1,0:T(8,128)(2,1)} %bitcast.36), channel_id=1, replica_groups=mesh['rep'=2,'fs_0'=2,'fs_1'=4,'fs_2'=4,'tp'=2] {'tp'}, dimensions={0} | all-to-all | bytes 6291456 | tf_op jit(solution)/shard_map/all_to_all | solution.py:27
  211.2 0.7 convert_reduce_fusion.1
  211.9 0.7 copy-done.3
  212.6 0.5 fusion.70
  213.1 0.7 multiply_reduce_fusion.1
  213.8 1.8 multiply_convert_fusion.3
  215.7 0.0 all-gather.13.cloned.1.call-update
  215.7 0.0 all-gather.17.cloned.1.call-start
  215.8 1.6 fusion.86
  217.4 0.0 all-gather.17.cloned.1.call-update
  217.4 42.8 %all-gather.15.cloned.1.call-done = bf16[4096,1024]{1,0:T(8,128)(2,1)} async-done(((bf16[64,1024]{1,0:T(8,128)(2,1)}), bf16[4096,1024]{1,0:T(8,128)(2,1)}) %all-gather.15.cloned.1.call-update) | async-done | bytes 8388624 | tf_op jit(solution)/shard_map/all_gather | solution.py:21
  260.2 16.5 %all-gather.13.cloned.1.call-done = bf16[768,2048]{1,0:T(8,128)(2,1)} async-done(((bf16[384,2048]{1,0:T(8,128)(2,1)}), bf16[768,2048]{1,0:T(8,128)(2,1)}) %all-gather.13.cloned.1.call-update) | async-done | bytes 3145744 | tf_op jit(solution)/shard_map/all_gather | solution.py:88
  276.7 6.7 %multiply_convert_fusion.1 = bf16[768,1024]{1,0:T(8,128)(2,1)S(1)} fusion(bf16[768,2048]{1,0:T(8,128)(2,1)} %all-gather.13.cloned.1.call-done, bf16[4096,1024]{1,0:T(8,128)(2,1)} %all-gather.15.cloned.1.call-done), kind=kOutput, calls=%fused_computation.14 | convolution fusion | flops 3223584768 | bytes 8912896 | tf_op jit(solution)/shard_map/dot_general | solution.py:48
  283.4 4.6 %multiply_convert_fusion.2 = bf16[768,1024]{1,0:T(8,128)(2,1)} fusion(bf16[768,2048]{1,0:T(8,128)(2,1)S(1)} %copy-done.9, bf16[4096,1024]{1,0:T(8,128)(2,1)S(1)} %copy-done.7), kind=kOutput, calls=%fused_computation.15 | convolution fusion | flops 3223584768 | bytes 8912896 | tf_op jit(solution)/shard_map/dot_general | solution.py:48
  288.0 70.6 %all-gather.17.cloned.1.call-done = bf16[4096,1024]{1,0:T(8,128)(2,1)} async-done(((bf16[64,1024]{1,0:T(8,128)(2,1)}), bf16[4096,1024]{1,0:T(8,128)(2,1)}) %all-gather.17.cloned.1.call-update) | async-done | bytes 8388624 | tf_op jit(solution)/shard_map/all_gather | solution.py:21
  358.6 5.4 %fusion = f32[768,2048]{1,0:T(8,128)S(1)} fusion(bf16[768,1024]{1,0:T(8,128)(2,1)S(1)} %multiply_convert_fusion.1, bf16[4096,1024]{1,0:T(8,128)(2,1)} %all-gather.17.cloned.1.call-done), kind=kOutput, calls=%fused_computation.4 | convolution fusion | flops 3221225472 | bytes 12058624 | tf_op jit(solution)/shard_map/dot_general | solution.py:52
  364.1 3.7 add_convert_fusion
  367.8 6.8 %all_to_all.11 = bf16[2,384,2048]{2,1,0:T(8,128)(2,1)S(1)} all-to-all(bf16[2,384,2048]{2,1,0:T(8,128)(2,1)S(1)} %bitcast.37), channel_id=1, replica_groups=mesh['rep'=2,'fs_0'=2,'fs_1'=4,'fs_2'=4,'tp'=2] {'tp'}, dimensions={0} | all-to-all | bytes 6291456 | tf_op jit(solution)/shard_map/all_to_all | solution.py:27
  374.6 0.7 convert_reduce_fusion
  375.3 0.7 copy-done.2
  376.0 0.5 fusion.71
  376.5 0.7 multiply_reduce_fusion
  377.2 1.8 multiply_convert_fusion
  (26 shorter events, 0.1 us)
Async XLA Ops:
  6.5 5.0 %copy-start = (f32[64,2048]{1,0:T(8,128)S(1)}, f32[64,2048]{1,0:T(8,128)}, u32[]{:S(2)}) copy-start(f32[64,2048]{1,0:T(8,128)} %param.17) | copy-start | bytes 1572868
  6.5 20.9 %all-gather.9.cloned.1.call-start = ((), (), s32[]{:S(2)}) async-start(), calls=%async_computation.3 | async-start | bytes 4718592 | tf_op jit(solution)/shard_map/all_gather | solution.py:68
  7.3 105.0 %all-gather.7.cloned.1.call-start = ((), (), s32[]{:S(2)}) async-start(), calls=%async_computation.2 | async-start | bytes 9584640 | tf_op jit(solution)/shard_map/all_gather | solution.py:21
  9.9 170.5 %all-gather.11.cloned.1.call-start = ((), (), s32[]{:S(2)}) async-start(), calls=%async_computation.4 | async-start | bytes 3194880 | tf_op jit(solution)/shard_map/all_gather | solution.py:21
  11.5 248.7 %all-gather.15.cloned.1.call-start = ((), (), s32[]{:S(2)}) async-start(), calls=%async_computation.6 | async-start | bytes 8519680 | tf_op jit(solution)/shard_map/all_gather | solution.py:21
  12.2 264.5 %all-gather.13.cloned.1.call-start = ((), (), s32[]{:S(2)}) async-start(), calls=%async_computation.5 | async-start | bytes 4718592 | tf_op jit(solution)/shard_map/all_gather | solution.py:88
  112.3 4.0 %copy-start.4 = (bf16[768,2048]{1,0:T(8,128)(2,1)S(1)}, bf16[768,2048]{1,0:T(8,128)(2,1)}, u32[]{:S(2)}) copy-start(bf16[768,2048]{1,0:T(8,128)(2,1)} %all-gather.9.cloned.1.call-done) | copy-start | bytes 9437188
  211.2 1.4 copy-start.3
  213.1 0.7 copy-start.5
  215.7 142.9 %all-gather.17.cloned.1.call-start = ((), (), s32[]{:S(2)}) async-start(), calls=%async_computation.7 | async-start | bytes 8519680 | tf_op jit(solution)/shard_map/all_gather | solution.py:21
  276.7 6.7 %copy-start.7 = (bf16[4096,1024]{1,0:T(8,128)(2,1)S(1)}, bf16[4096,1024]{1,0:T(8,128)(2,1)}, u32[]{:S(2)}) copy-start(bf16[4096,1024]{1,0:T(8,128)(2,1)} %all-gather.15.cloned.1.call-done) | copy-start | bytes 25165828
  276.7 6.7 %copy-start.9 = (bf16[768,2048]{1,0:T(8,128)(2,1)S(1)}, bf16[768,2048]{1,0:T(8,128)(2,1)}, u32[]{:S(2)}) copy-start(bf16[768,2048]{1,0:T(8,128)(2,1)} %all-gather.13.cloned.1.call-done) | copy-start | bytes 9437188
  358.6 5.4 %copy-start.8 = (bf16[4096,1024]{1,0:T(8,128)(2,1)S(1)}, bf16[4096,1024]{1,0:T(8,128)(2,1)}, u32[]{:S(2)}) copy-start(bf16[4096,1024]{1,0:T(8,128)(2,1)} %all-gather.17.cloned.1.call-done) | copy-start | bytes 25165828
  358.6 5.4 %copy-start.10 = (bf16[768,1024]{1,0:T(8,128)(2,1)S(1)}, bf16[768,1024]{1,0:T(8,128)(2,1)}, u32[]{:S(2)}) copy-start(bf16[768,1024]{1,0:T(8,128)(2,1)} %multiply_convert_fusion.2) | copy-start | bytes 4718596
  374.6 1.4 copy-start.2
  376.5 0.7 copy-start.6
  377.2 1.9 copy-start.1
Sparse Core Ops, SparseCore 0:
  9.0 18.4 all-gather.8
  30.2 82.0 all-gather.6
  115.1 65.2 all-gather.10
  183.1 77.0 all-gather.14
  261.7 14.9 all-gather.12
  279.4 79.1 all-gather.16
where the time goes:
time: 386 us
  waiting for transfers between devices  282 us (73%)
  matrix products  54.6 us (14%)
  blocking collectives  16.1 us (4%)
  between operations  13.7 us (4%)
  local copies, waits for them, and re-layouts  11.4 us (3%)
  other arithmetic  8.22 us (2%)
    all_gather x4, waiting for transfers between devices, gathered_halves(): full = lax.all_gather(x, REP_FS, axis=0, tiled=True)  250 us
    dot_general x4, matrix products, dot_t(): lax.dot_general(a, b, (((1,), (1,)), ((), ())), preferred_element_type=jn...  30.7 us
    dot_general x6, matrix products, dot(): return jnp.dot(a, b, preferred_element_type=jnp.float32)  24 us
    all_gather x1, waiting for transfers between devices, local(): grouped_first = lax.all_gather(first, 'tp', axis=0, tiled=True)  16.5 us
    all_to_all x2, blocking collectives, sum_at_owner(): lax.all_to_all(tiles, axis, split_axis=0, concat_axis=0, tiled=True)  16.1 us
    all_gather x1, waiting for transfers between devices, local(): grouped = lax.all_gather(tokens, 'tp', axis=0, tiled=True)  14.3 us
  transfers between devices with their start and end apart: 6, of which 6 were waited for; matrix products, arithmetic and copies ran while one was open for 16% of the time, Pallas kernels for 0%

commit v1 on v0

--- a/solution.py
+++ b/solution.py
@@ -1,3 +1,4 @@
+import functools
 import jax
 import jax.numpy as jnp
 from jax import lax
@@ -10,6 +11,16 @@
 REP_FS_TP = ("rep", "fs_0", "fs_1", "fs_2", "tp")
 residual_scale = 2.0**0.25
 norm_epsilon = 1e-05
+
+
+def proceed_runs(packet, group_axis):
+    seen_now = jax.lax.psum(1, axis_name=group_axis)
+    moved = jnp.stack([packet] * seen_now, axis=0)
+    formed = jax.lax.all_to_all(moved, axis_name=group_axis, split_axis=0, concat_axis=0)
+    return jnp.concatenate(formed, axis=0)
+
+
+view_the_levels_all = functools.partial(proceed_runs, group_axis="tp")
 
 
 def own_half(x, dim):
@@ -85,7 +96,7 @@
         mixing = mixing + dot_t(mixed, mixout_full[h])
     mixing = sum_at_owner(mixing.astype(bf), "tp")
     first = layer_norm(residual_scale * tokens.astype(jnp.float32) + mixing, norm_first).astype(bf)
-    grouped_first = lax.all_gather(first, "tp", axis=0, tiled=True)
+    grouped_first = view_the_levels_all(first)
     lowered = 0.0
     for h in range(2):
         raised = jax.nn.relu(dot(grouped_first, up_full[h]))

time: 386 us -> 368 us (0.953)
  waiting for transfers between devices: 282 us -> 255 us
  starting transfers between devices: 0.21 us -> 5.79 us
    all_gather x1 -> x0, waiting for transfers between devices: 16.5 us -> none  [local(): grouped_first = lax.all_gather(first, 'tp', axis=0, tiled=True)]
    all_gather x4, waiting for transfers between devices: 250 us -> 241 us  [gathered_halves(): full = lax.all_gather(x, REP_FS, axis=0, tiled=True)]
    all_to_all x0 -> x1, starting transfers between devices: none -> 5.63 us  [proceed_runs(): jax.lax.all_to_all(moved, axis_name=group_axis, split_axis=0, concat_axis=0)]
  transfers between devices with their start and end apart: 6 -> 6, of which waited for: 6 -> 5; matrix products, arithmetic and copies ran while one was open for 16% -> 17% of each run, Pallas kernels for 0% -> 0%
where the time goes in v1:
time: 368 us
  waiting for transfers between devices  255 us (69%)
  matrix products  58.1 us (16%)
  blocking collectives  16 us (4%)
  between operations  13.3 us (4%)
  local copies, waits for them, and re-layouts  9.99 us (3%)
  other arithmetic  9.04 us (2%)
  starting transfers between devices  5.79 us (2%)
    all_gather x4, waiting for transfers between devices, gathered_halves(): full = lax.all_gather(x, REP_FS, axis=0, tiled=True)  241 us
    dot_general x4, matrix products, dot_t(): lax.dot_general(a, b, (((1,), (1,)), ((), ())), preferred_element_type=jn...  31.2 us
    dot_general x6, matrix products, dot(): return jnp.dot(a, b, preferred_element_type=jnp.float32)  26.9 us
    all_to_all x2, blocking collectives, sum_at_owner(): lax.all_to_all(tiles, axis, split_axis=0, concat_axis=0, tiled=True)  16 us
    all_gather x1, waiting for transfers between devices, local(): grouped = lax.all_gather(tokens, 'tp', axis=0, tiled=True)  13.5 us
  transfers between devices with their start and end apart: 6, of which 5 were waited for; matrix products, arithmetic and copies ran while one was open for 17% of the time, Pallas kernels for 0%

profile of v1, /device:TPU:1, one launch (start us, length us, event | category | flops | bytes accessed | tf_op | source)
XLA Modules:
  0.0 367.6 jit_solution(9069098653794527446)
XLA Ops:
  6.5 0.0 copy-start
  6.5 0.0 all-gather.8.cloned.1.call-start
  6.5 0.7 all-gather.8.cloned.1.call-update
  7.3 0.0 all-gather.6.cloned.1.call-start
  7.3 0.9 dynamic-slice_convert_fusion.5
  8.2 1.0 dynamic-slice_convert_fusion.3
  9.2 0.7 pad_maximum_fusion.1
  9.9 0.0 all-gather.6.cloned.1.call-update
  9.9 0.0 all-gather.10.cloned.1.call-start
  9.9 1.5 fusion.87
  11.4 0.0 all-gather.10.cloned.1.call-update
  11.5 0.0 all-gather.12.cloned.1.call-start
  11.5 0.7 dynamic-slice_convert_fusion.1
  12.2 0.0 all-gather.12.cloned.1.call-update
  12.2 0.0 all-gather.14.cloned.1.call-start
  12.3 1.6 fusion.86
  13.9 0.0 all-gather.14.cloned.1.call-update
  14.0 13.5 %all-gather.8.cloned.1.call-done = bf16[768,2048]{1,0:T(8,128)(2,1)} async-done(((bf16[384,2048]{1,0:T(8,128)(2,1)}), bf16[768,2048]{1,0:T(8,128)(2,1)}) %all-gather.8.cloned.1.call-update) | async-done | bytes 3145744 | tf_op jit(solution)/shard_map/all_gather | solution.py:79
  27.5 84.8 %all-gather.6.cloned.1.call-done = bf16[4096,1152]{1,0:T(8,128)(2,1)} async-done(((bf16[64,1152]{1,0:T(8,128)(2,1)}), bf16[4096,1152]{1,0:T(8,128)(2,1)}) %all-gather.6.cloned.1.call-update) | async-done | bytes 9437200 | tf_op jit(solution)/shard_map/all_gather | solution.py:32
  112.3 4.0 %fusion.23 = f32[384,768]{1,0:T(8,128)S(1)} fusion(bf16[768,2048]{1,0:T(8,128)(2,1)} %all-gather.8.cloned.1.call-done, bf16[4096,1152]{1,0:T(8,128)(2,1)} %all-gather.6.cloned.1.call-done), kind=kOutput, calls=%fused_computation.30 | convolution fusion | flops 1207959552 | bytes 5898240 | tf_op jit(solution)/shard_map/dot_general | solution.py:59
  116.3 2.9 fusion.50
  119.2 1.7 fusion.96
  120.9 2.9 fusion.15
  123.9 2.9 fusion.47
  126.8 1.8 fusion.95
  128.6 51.7 %all-gather.10.cloned.1.call-done = bf16[4096,384]{1,0:T(8,128)(2,1)} async-done(((bf16[64,384]{1,0:T(8,128)(2,1)}), bf16[4096,384]{1,0:T(8,128)(2,1)}) %all-gather.10.cloned.1.call-update) | async-done | bytes 3145744 | tf_op jit(solution)/shard_map/all_gather | solution.py:32
  180.3 10.3 %fusion.21 = f32[768,2048]{1,0:T(8,128)} fusion(bf16[4096,384]{1,0:T(8,128)(2,1)} %all-gather.10.cloned.1.call-done, bf16[768,2048]{1,0:T(8,128)(2,1)} %all-gather.8.cloned.1.call-done, bf16[4096,1152]{1,0:T(8,128)(2,1)} %all-gather.6.cloned.1.call-done, f32[767,384]{0,1:T(8,128)} %get-tuple-element.14, f32[768,384]{0,1:T(8,128)S(1)} %fusion.50, ...), kind=kOutput, calls=%fused_computation.28 | convolution fusion | flops 2418573312 | bytes 16128000 | tf_op jit(solution)/shard_map/dot_general | solution.py:63
  190.6 11.4 %add_convert_fusion.1 = bf16[768,2048]{1,0:T(8,128)(2,1)} fusion(f32[768,2048]{1,0:T(8,128)} %fusion.21, bf16[4096,384]{1,0:T(8,128)(2,1)} %all-gather.10.cloned.1.call-done, bf16[768,2048]{1,0:T(8,128)(2,1)} %all-gather.8.cloned.1.call-done, bf16[4096,1152]{1,0:T(8,128)(2,1)} %all-gather.6.cloned.1.call-done, f32[767,384]{0,1:T(8,128)} %get-tuple-element.12, ...), kind=kOutput, calls=%fused_computation.3 | convolution fusion | flops 2421719040 | bytes 19273728 | tf_op jit(solution)/shard_map/dot_general | solution.py:63
  202.0 9.3 %all_to_all.15 = bf16[2,384,2048]{2,1,0:T(8,128)(2,1)S(1)} all-to-all(bf16[2,384,2048]{2,1,0:T(8,128)(2,1)} %bitcast.39), channel_id=1, replica_groups=mesh['rep'=2,'fs_0'=2,'fs_1'=4,'fs_2'=4,'tp'=2] {'tp'}, dimensions={0} | all-to-all | bytes 6291456 | tf_op jit(solution)/shard_map/all_to_all | solution.py:38
  211.3 0.7 convert_reduce_fusion.1
  212.0 0.7 copy-done.2
  212.7 0.5 fusion.70
  213.2 0.7 multiply_reduce_fusion.1
  213.9 0.7 multiply_convert_fusion.3
  214.6 2.0 pad_maximum_fusion
  216.6 5.6 %all-to-all-start.1 = ((bf16[2,384,2048]{2,1,0:T(8,128)(2,1)}), bf16[2,384,2048]{2,1,0:T(8,128)(2,1)}, u32[]{:S(2)}, u32[]{:S(2)}) async-start(bf16[2,384,2048]{2,1,0:T(8,128)(2,1)} %pad_maximum_fusion), calls=%async_computation.1 | async-start | bytes 6291456 | tf_op jit(solution)/shard_map/all_to_all | solution.py:19
  222.2 38.0 %all-gather.12.cloned.1.call-done = bf16[4096,1024]{1,0:T(8,128)(2,1)} async-done(((bf16[64,1024]{1,0:T(8,128)(2,1)}), bf16[4096,1024]{1,0:T(8,128)(2,1)}) %all-gather.12.cloned.1.call-update) | async-done | bytes 8388624 | tf_op jit(solution)/shard_map/all_gather | solution.py:32
  260.2 0.0 all-to-all-done.1
  260.2 7.8 %multiply_convert_fusion.1 = bf16[768,1024]{1,0:T(8,128)(2,1)} fusion(bf16[768,2048]{1,0:T(8,128)(2,1)} %bitcast.7, bf16[4096,1024]{1,0:T(8,128)(2,1)} %all-gather.12.cloned.1.call-done), kind=kOutput, calls=%fused_computation.15 | convolution fusion | flops 3223584768 | bytes 8912896 | tf_op jit(solution)/shard_map/dot_general | solution.py:59
  268.0 6.4 %multiply_convert_fusion.2 = bf16[768,1024]{1,0:T(8,128)(2,1)} fusion(bf16[768,2048]{1,0:T(8,128)(2,1)} %bitcast.7, bf16[4096,1024]{1,0:T(8,128)(2,1)S(1)} %copy-done.7), kind=kOutput, calls=%fused_computation.16 | convolution fusion | flops 3223584768 | bytes 8912896 | tf_op jit(solution)/shard_map/dot_general | solution.py:59
  274.4 66.4 %all-gather.14.cloned.1.call-done = bf16[4096,1024]{1,0:T(8,128)(2,1)} async-done(((bf16[64,1024]{1,0:T(8,128)(2,1)}), bf16[4096,1024]{1,0:T(8,128)(2,1)}) %all-gather.14.cloned.1.call-update) | async-done | bytes 8388624 | tf_op jit(solution)/shard_map/all_gather | solution.py:32
  340.9 5.9 %fusion = f32[768,2048]{1,0:T(8,128)S(1)} fusion(bf16[768,1024]{1,0:T(8,128)(2,1)} %multiply_convert_fusion.1, bf16[4096,1024]{1,0:T(8,128)(2,1)} %all-gather.14.cloned.1.call-done), kind=kOutput, calls=%fused_computation.4 | convolution fusion | flops 3221225472 | bytes 12058624 | tf_op jit(solution)/shard_map/dot_general | solution.py:63
  346.8 3.7 %add_convert_fusion = bf16[768,2048]{1,0:T(8,128)(2,1)S(1)} fusion(f32[768,2048]{1,0:T(8,128)S(1)} %fusion, bf16[768,1024]{1,0:T(8,128)(2,1)S(1)} %copy-done.9, bf16[4096,1024]{1,0:T(8,128)(2,1)S(1)} %copy-done.8), kind=kOutput, calls=%fused_computation.1 | convolution fusion | flops 3224371200 | bytes 15204352 | tf_op jit(solution)/shard_map/dot_general | solution.py:63
  350.5 6.7 %all_to_all.16 = bf16[2,384,2048]{2,1,0:T(8,128)(2,1)S(1)} all-to-all(bf16[2,384,2048]{2,1,0:T(8,128)(2,1)S(1)} %bitcast.40), channel_id=1, replica_groups=mesh['rep'=2,'fs_0'=2,'fs_1'=4,'fs_2'=4,'tp'=2] {'tp'}, dimensions={0} | all-to-all | bytes 6291456 | tf_op jit(solution)/shard_map/all_to_all | solution.py:38
  357.2 0.7 convert_reduce_fusion
  358.0 0.5 fusion.71
  358.5 0.7 multiply_reduce_fusion
  359.2 1.8 multiply_convert_fusion
  (24 shorter events, 0.1 us)
Async XLA Ops:
  6.5 5.0 %copy-start = (f32[64,2048]{1,0:T(8,128)S(1)}, f32[64,2048]{1,0:T(8,128)}, u32[]{:S(2)}) copy-start(f32[64,2048]{1,0:T(8,128)} %param.17) | copy-start | bytes 1572868
  6.5 7.4 %copy-start.6 = (f32[3,768]{1,0:T(4,128)S(1)}, f32[3,768]{1,0:T(4,128)}, u32[]{:S(2)}) copy-start(f32[3,768]{1,0:T(4,128)} %param.14) | copy-start | bytes 27652
  6.5 20.9 %all-gather.8.cloned.1.call-start = ((), (), s32[]{:S(2)}) async-start(), calls=%async_computation.4 | async-start | bytes 4718592 | tf_op jit(solution)/shard_map/all_gather | solution.py:79
  7.3 105.0 %all-gather.6.cloned.1.call-start = ((), (), s32[]{:S(2)}) async-start(), calls=%async_computation.3 | async-start | bytes 9584640 | tf_op jit(solution)/shard_map/all_gather | solution.py:32
  9.9 170.5 %all-gather.10.cloned.1.call-start = ((), (), s32[]{:S(2)}) async-start(), calls=%async_computation.5 | async-start | bytes 3194880 | tf_op jit(solution)/shard_map/all_gather | solution.py:32
  11.5 248.7 %all-gather.12.cloned.1.call-start = ((), (), s32[]{:S(2)}) async-start(), calls=%async_computation.6 | async-start | bytes 8519680 | tf_op jit(solution)/shard_map/all_gather | solution.py:32
  12.2 328.7 %all-gather.14.cloned.1.call-start = ((), (), s32[]{:S(2)}) async-start(), calls=%async_computation.7 | async-start | bytes 8519680 | tf_op jit(solution)/shard_map/all_gather | solution.py:32
  112.3 4.0 %copy-start.3 = (bf16[768,2048]{1,0:T(8,128)(2,1)S(1)}, bf16[768,2048]{1,0:T(8,128)(2,1)}, u32[]{:S(2)}) copy-start(bf16[768,2048]{1,0:T(8,128)(2,1)} %all-gather.8.cloned.1.call-done) | copy-start | bytes 9437188
  211.2 1.4 copy-start.2
  213.1 0.7 copy-start.4
  216.6 43.7 %all-to-all-start.1 = ((bf16[2,384,2048]{2,1,0:T(8,128)(2,1)}), bf16[2,384,2048]{2,1,0:T(8,128)(2,1)}, u32[]{:S(2)}, u32[]{:S(2)}) async-start(bf16[2,384,2048]{2,1,0:T(8,128)(2,1)} %pad_maximum_fusion), calls=%async_computation.1 | async-start | bytes 6291456 | tf_op jit(solution)/shard_map/all_to_all | solution.py:19
  260.2 7.8 %copy-start.7 = (bf16[4096,1024]{1,0:T(8,128)(2,1)S(1)}, bf16[4096,1024]{1,0:T(8,128)(2,1)}, u32[]{:S(2)}) copy-start(bf16[4096,1024]{1,0:T(8,128)(2,1)} %all-gather.12.cloned.1.call-done) | copy-start | bytes 25165828
  340.9 5.9 %copy-start.8 = (bf16[4096,1024]{1,0:T(8,128)(2,1)S(1)}, bf16[4096,1024]{1,0:T(8,128)(2,1)}, u32[]{:S(2)}) copy-start(bf16[4096,1024]{1,0:T(8,128)(2,1)} %all-gather.14.cloned.1.call-done) | copy-start | bytes 25165828
  340.9 5.9 %copy-start.9 = (bf16[768,1024]{1,0:T(8,128)(2,1)S(1)}, bf16[768,1024]{1,0:T(8,128)(2,1)}, u32[]{:S(2)}) copy-start(bf16[768,1024]{1,0:T(8,128)(2,1)} %multiply_convert_fusion.2) | copy-start | bytes 4718596
  358.4 0.7 copy-start.5
  359.2 1.9 copy-start.1
Sparse Core Ops, SparseCore 0:
  9.0 18.4 all-gather.7
  30.2 82.0 all-gather.5
  115.1 65.2 all-gather.9
  183.1 77.0 all-gather.11
  262.9 77.9 all-gather.13
